TPU v7x, 32 devices: a whole 2x2x4 slice. The times are simulated.
32 devices in a mesh: ep: 8 (over z, core), tp: 4 (over y, x).
Axes of the slice: x: 2, y: 2, z: 4, core: 2. Of those that a mesh axis runs over, the one named last changes fastest.
Arguments:
- query_rows: bfloat16 [3072, 2048], P('ep', 'tp'), may hold values from -6 to 6
- key_rows: bfloat16 [3072, 2048], P('ep', 'tp'), may hold values from -6 to 6
- value_rows: bfloat16 [3072, 2048], P('ep', 'tp'), may hold values from -6 to 6
- second_scale: float32 [16], P('tp'), may hold values from 0.3 to 0.8
- head_gain: float32 [128], replicated, may hold values from 0.1 to 1.9
- out_weight: bfloat16 [2048, 4096], P(None, 'tp'), may hold values from -0.125 to 0.125
- routed_rows: bfloat16 [1024, 4096], P('ep', 'tp'), may hold values from -6 to 6
- norm_gain: float32 [4096], replicated, may hold values from 0.1 to 1.9
- route_ids: int32 [1024, 2], P('ep'), may hold values from 0 to 7, all different within a row; in each aligned block of 128 rows (0 to 127, 128 to 255, ...) at most 64 rows name the same one
- route_weight: float32 [1024, 2], P('ep'), may hold values from 0.1 to 0.9
- expert_gate: bfloat16 [8, 4096, 2048], P('ep', None, 'tp'), may hold values from -0.09375 to 0.09375
- expert_up: bfloat16 [8, 4096, 2048], P('ep', None, 'tp'), may hold values from -0.09375 to 0.09375
- expert_down: bfloat16 [8, 2048, 4096], P('ep', None, 'tp'), may hold values from -0.125 to 0.125
Outputs:
- mixer_out: bfloat16 [3072, 4096], P('ep', 'tp')
- expert_mix: bfloat16 [1024, 4096], P('ep', 'tp')
Inputs may be any that keep to these rules, and one draw needn't show every extreme that they name: `route_ids`: among the 128 tokens of one index of ep, no expert is named by more than 64 of them, a bound that some block reaches.
All inputs are finite; a program needn't handle non-finite values.
Results may differ from a plain program's by a relative error of at most 0.0085.
Values may be sent and summed in bfloat16 or wider, within the bound.
A program may use at most 128 MiB of HBM per device.

v0:
```python
import functools

import jax
import jax.numpy as jnp
from jax import lax
from jax.experimental import pallas as pl
from jax.experimental.pallas import tpu as pltpu
from jax.sharding import PartitionSpec as P

eps = 1e-06
head_factor = 0.8
neg_big = -1e30
lanes = 2
f32 = jnp.float32
bf16 = jnp.bfloat16


def dot(a, b):
    return jnp.dot(a, b, preferred_element_type=f32)


def layer_kernel(
    n_ep,
    n_tp,
    scale_ref,
    q_hbm,
    k_hbm,
    v_hbm,
    gain_ref,
    wo_hbm,
    rows_hbm,
    norm_ref,
    ids_ref,
    route_w_ref,
    wg_hbm,
    wu_hbm,
    wd_hbm,
    mixer_ref,
    mix_ref,
    q_in,
    q_two,
    k_all,
    v_all,
    rows_all,
    ids_all,
    arr,
    normed,
    hid_all,
    out_e,
    ret,
    head_all,
    spread,
    acc,
    run_max,
    run_sum,
    wg,
    wu,
    wd,
    wo,
    local_sem,
    weight_sem,
    rows_up,
    rows_down,
    rows_side,
    rows_recv,
    ids_send,
    ids_recv,
    kv_up,
    kv_side,
    kv_recv,
    arr_send,
    arr_recv,
    hid_send,
    hid_recv,
    head_send,
    head_recv,
    ret_send,
    ret_recv,
):
    e = lax.axis_index("ep")
    t = lax.axis_index("tp")
    n_z = n_ep // lanes
    z = lax.div(e, lanes)
    c = lax.rem(e, lanes)
    partner = z * lanes + (1 - c)
    n_tok = q_in.shape[0]
    tok_b = rows_all.shape[1]
    per_head = acc.shape[0]
    head_w = q_two.shape[2]
    val_w = acc.shape[2]
    slots, out_w = ret.shape
    cap = slots // n_ep
    half = n_z // 2
    cols = arr.shape[2]
    hidden_w = hid_all.shape[2]
    route_count = ids_ref.shape[0]

    def remote(src, dst, send, recv, ep_to, tp_to):
        return pltpu.make_async_remote_copy(
            src_ref=src,
            dst_ref=dst,
            send_sem=send,
            recv_sem=recv,
            device_id=(ep_to, tp_to),
            device_id_type=pl.DeviceIdType.MESH,
        )

    loads = [
        pltpu.make_async_copy(rows_hbm, rows_all.at[e], local_sem.at[0]),
        pltpu.make_async_copy(k_hbm, k_all.at[e], local_sem.at[1]),
        pltpu.make_async_copy(v_hbm, v_all.at[e], local_sem.at[2]),
        pltpu.make_async_copy(q_hbm, q_in, local_sem.at[3]),
    ]
    for load in loads:
        load.start()
    ids_all[e, pl.ds(0, route_count)] = ids_ref[...]
    weights = [
        pltpu.make_async_copy(wg_hbm.at[0], wg, weight_sem.at[0]),
        pltpu.make_async_copy(wu_hbm.at[0], wu, weight_sem.at[1]),
        pltpu.make_async_copy(wd_hbm.at[0], wd, weight_sem.at[2]),
        pltpu.make_async_copy(wo_hbm, wo, weight_sem.at[3]),
    ]

    barrier = pltpu.get_barrier_semaphore()

    def greet_ep(i, carry):
        to = lax.rem(e + i, n_ep)
        pl.semaphore_signal(barrier, inc=1, device_id=(to, t), device_id_type=pl.DeviceIdType.MESH)
        return carry

    def greet_tp(i, carry):
        to = lax.rem(t + i, n_tp)
        pl.semaphore_signal(barrier, inc=1, device_id=(e, to), device_id_type=pl.DeviceIdType.MESH)
        return carry

    lax.fori_loop(1, n_ep, greet_ep, 0)
    lax.fori_loop(1, n_tp, greet_tp, 0)
    pl.semaphore_wait(barrier, n_ep - 1 + n_tp - 1)
    for load in loads:
        load.wait()

    def ids_copy(to):
        return remote(ids_all.at[e], ids_all.at[e], ids_send.at[to], ids_recv.at[e], to, t)

    def ids_arrival(b):
        return remote(ids_all.at[b], ids_all.at[b], ids_send.at[b], ids_recv.at[b], b, t)

    def rows_copy(block, send, to):
        return remote(rows_all.at[block], rows_all.at[block], send, rows_recv.at[block], to, t)

    def rows_copy_up(j):
        return rows_copy(j * lanes + c, rows_up.at[j], lax.rem(e + lanes, n_ep))

    def rows_copy_down(j):
        return rows_copy(j * lanes + c, rows_down.at[j], lax.rem(e + n_ep - lanes, n_ep))

    def rows_copy_side(j):
        return rows_copy(j * lanes + c, rows_side.at[j], partner)

    def kv_copies(j, sems, to):
        block = j * lanes + c
        return [
            remote(ref.at[block], ref.at[block], sems.at[i, j], kv_recv.at[i, block], to, t)
            for i, ref in enumerate((k_all, v_all))
        ]

    def kv_copies_up(j):
        return kv_copies(j, kv_up, lax.rem(e + lanes, n_ep))

    def kv_copies_side(j):
        return kv_copies(j, kv_side, partner)

    def kv_wait(block):
        for i, ref in enumerate((k_all, v_all)):
            remote(
                ref.at[block], ref.at[block], kv_up.at[i, 0], kv_recv.at[i, block], partner, t
            ).wait_recv()

    square = n_tp == 4
    across = t + 1 - 2 * lax.rem(t, 2)
    along = lax.rem(t + 2, n_tp)
    corner = n_tp - 1 - t

    def piece(buf, source, i, units):
        step = buf.shape[1] // (2 * units)
        return buf.at[source, pl.ds(i * step, step)]

    def tp_copy(buf, sems, units, source, i, row, to):
        ref = piece(buf, source, i, units)
        return remote(ref, ref, sems[0].at[row, i], sems[1].at[source, i], e, to)

    def tp_peers(work):
        def one(i, carry):
            to = lax.rem(t + i, n_tp)
            work(to, to)
            return carry

        if square:
            work(across, 0)
            work(along, 1)
        else:
            lax.fori_loop(1, n_tp, one, 0)

    def tp_send(buf, sems, units, unit):
        for i in (2 * unit, 2 * unit + 1):
            tp_peers(lambda to, row: tp_copy(buf, sems, units, t, i, row, to).start())

    def tp_hand_on(buf, sems, units, unit):
        if square:
            i = 2 * unit
            tp_copy(buf, sems, units, across, i, 2, across).wait_recv()
            tp_copy(buf, sems, units, across, i, 2, along).start()
            tp_copy(buf, sems, units, along, i + 1, 2, along).wait_recv()
            tp_copy(buf, sems, units, along, i + 1, 2, across).start()

    def tp_arrive(buf, sems, units, unit):
        i = 2 * unit
        if square:
            for source, at in ((across, i + 1), (along, i), (corner, i), (corner, i + 1)):
                tp_copy(buf, sems, units, source, at, 2, source).wait_recv()
        else:
            for at in (i, i + 1):
                tp_peers(lambda to, row: tp_copy(buf, sems, units, to, at, row, to).wait_recv())

    def tp_drain(buf, sems, units):
        for i in range(2 * units):
            tp_peers(lambda to, row: tp_copy(buf, sems, units, t, i, row, to).wait_send())
            if square:
                source, to = (across, along) if i % 2 == 0 else (along, across)
                tp_copy(buf, sems, units, source, i, 2, to).wait_send()

    arr_sems = (arr_send, arr_recv)
    hid_sems = (hid_send, hid_recv)
    head_sems = (head_send, head_recv)

    def unit_of(j):
        return lax.rem(lax.div(j, half) + lax.div(z, half), 2)

    def first_slot(j, side):
        return pl.multiple_of(((unit_of(j) * 2 + side) * half + lax.rem(j, half)) * cap, cap)

    def ret_part(b):
        return ret.at[pl.ds(pl.multiple_of(b * cap, cap), cap)]

    def ret_copy(j, side):
        to = j * lanes + (c if side == 0 else 1 - c)
        return remote(
            out_e.at[pl.ds(first_slot(j, side), cap)],
            ret_part(e),
            ret_send.at[to],
            ret_recv.at[e],
            to,
            t,
        )

    def ret_each(unit, work):
        def one(i, carry):
            j = lax.rem(lax.div(z, half) + unit, 2) * half + i
            if unit == 0:

                @pl.when(j != z)
                def _():
                    work(ret_copy(j, 0))

            else:
                work(ret_copy(j, 0))
            work(ret_copy(j, 1))
            return carry

        lax.fori_loop(0, half, one, 0)

    def ret_arrival(b):
        return remote(ret_part(b), ret_part(b), ret_send.at[b], ret_recv.at[b], b, t)

    def each_ep(work):
        def one(i, carry):
            work(lax.rem(e + i, n_ep))
            return carry

        lax.fori_loop(1, n_ep, one, 0)

    each_ep(lambda to: ids_copy(to).start())

    def pick(block, j, side):
        ids = ids_all[block]
        hit = (ids[0:1] == e).astype(f32)
        for k in range(1, route_count):
            hit = hit + (ids[k : k + 1] == e).astype(f32)
        before = (
            lax.broadcasted_iota(jnp.int32, (tok_b, tok_b), 0)
            < lax.broadcasted_iota(jnp.int32, (tok_b, tok_b), 1)
        ).astype(bf16)
        ranks = dot(jnp.broadcast_to(hit, (16, tok_b)).astype(bf16), before)[0:1]
        slot = lax.broadcasted_iota(jnp.int32, (cap, tok_b), 0).astype(f32)
        chosen = jnp.where((slot == ranks) & (hit > 0.5), 1.0, 0.0).astype(bf16)
        start = first_slot(j, side)
        i = unit_of(j) * 2 + side
        arr[t, pl.ds(start, cap)] = dot(chosen, rows_all[block]).astype(bf16)
        part = arr.at[t, pl.ds(start, cap)]
        tp_peers(
            lambda to, row: remote(
                part, part, arr_send.at[row, i], arr_recv.at[t, i], e, to
            ).start()
        )

    def rows_step(s, carry):
        low, high = z - s, z + s

        @pl.when((s > 0) & (low >= 0))
        def _():
            rows_copy_down(low).wait_recv()

        @pl.when((low >= 0) & (z + 1 < n_z))
        def _():
            rows_copy_up(low).start()

        @pl.when((s > 0) & (high < n_z))
        def _():
            rows_copy_up(high).wait_recv()

        @pl.when((high < n_z) & (z > 0))
        def _():
            rows_copy_down(high).start()

        @pl.when((s == z) & (z + 1 < n_z))
        def _():
            for copy in kv_copies_up(z):
                copy.start()

        @pl.when((s == z) & (c == 0))
        def _():
            for copy in kv_copies_side(z):
                copy.start()

        @pl.when(low >= 0)
        def _():
            rows_copy_side(low).start()

        @pl.when((s > 0) & (high < n_z))
        def _():
            rows_copy_side(high).start()

        def take(j):
            mine, other = j * lanes + c, j * lanes + (1 - c)

            @pl.when(j != z)
            def _():
                ids_arrival(mine).wait_recv()

            pick(mine, j, 0)
            ids_arrival(other).wait_recv()
            rows_copy(other, rows_side.at[j], partner).wait_recv()
            pick(other, j, 1)

        @pl.when(low >= 0)
        def _():
            take(low)

        @pl.when((s > 0) & (high < n_z))
        def _():
            take(high)

        return carry

    lax.fori_loop(0, n_z, rows_step, 0)
    for weight in weights:
        weight.start()
    tp_hand_on(arr, arr_sems, 2, 0)

    lane = lax.broadcasted_iota(jnp.int32, (n_tok, head_w), 1)

    def split_maps(h, carry):
        scaled = q_in[:, pl.ds(pl.multiple_of(h * head_w, head_w), head_w)].astype(f32) * (
            (head_w // 2) ** -0.5
        )
        q_two[h, pl.ds(0, n_tok)] = jnp.where(lane < head_w // 2, scaled, 0.0).astype(bf16)
        q_two[h, pl.ds(n_tok, n_tok)] = jnp.where(lane < head_w // 2, 0.0, scaled).astype(bf16)
        return carry

    lax.fori_loop(0, per_head, split_maps, 0)

    def attend(block, own):
        def one(h, carry):
            keys = k_all[block, :, pl.ds(pl.multiple_of(h * head_w, head_w), head_w)]
            values = v_all[block, :, pl.ds(pl.multiple_of(h * val_w, val_w), val_w)]
            for m in range(2):
                part = pl.ds(m * n_tok, n_tok)
                scores = lax.dot_general(
                    q_two[h, part], keys, (((1,), (1,)), ((), ())), preferred_element_type=f32
                )
                if own:
                    scores = jnp.where(
                        lax.broadcasted_iota(jnp.int32, (n_tok, n_tok), 0)
                        >= lax.broadcasted_iota(jnp.int32, (n_tok, n_tok), 1),
                        scores,
                        neg_big,
                    )
                top = jnp.max(scores, axis=-1, keepdims=True)
                if not own:
                    old = run_max[h, part]
                    top = jnp.maximum(old, top)
                shares = jnp.exp(scores - top)
                total = jnp.sum(shares, axis=-1, keepdims=True)
                update = dot(shares.astype(bf16), values)
                if not own:
                    shrink = jnp.exp(old - top)
                    total = total + run_sum[h, part] * shrink
                    update = update + acc[h, part] * shrink
                run_max[h, part] = top
                run_sum[h, part] = total
                acc[h, part] = update
            return carry

        lax.fori_loop(0, per_head, one, 0)

    attend(e, True)

    @pl.when(c == 1)
    def _():
        kv_wait(partner)
        attend(partner, False)

    tp_hand_on(arr, arr_sems, 2, 1)

    def kv_pass(s, carry):
        j = z - s

        @pl.when(j >= 0)
        def _():
            kv_wait(j * lanes + c)

            @pl.when(z + 1 < n_z)
            def _():
                for copy in kv_copies_up(j):
                    copy.start()

            for copy in kv_copies_side(j):
                copy.start()

        return carry

    def kv_attend(s, carry):
        j = z - s

        @pl.when(j >= 0)
        def _():
            attend(j * lanes + c, False)
            kv_wait(j * lanes + (1 - c))
            attend(j * lanes + (1 - c), False)

        return carry

    lax.fori_loop(1, 2, kv_pass, 0)

    for weight in weights:
        weight.wait()
    unit_rows = slots // 2
    n_rows = min(unit_rows, 64)
    tile_f = min(hidden_w, 256)

    def expert_in(unit):
        tp_arrive(arr, arr_sems, 2, unit)

        def norm_step(i, carry):
            part = pl.ds(pl.multiple_of(unit * unit_rows + i * n_rows, n_rows), n_rows)
            squares = jnp.zeros((n_rows, 1), f32)
            for p in range(n_tp):
                x = arr[p, part].astype(f32)
                squares = squares + jnp.sum(x * x, axis=-1, keepdims=True)
            factor = lax.rsqrt(squares / (n_tp * cols) + eps)
            for p in range(n_tp):
                where = pl.ds(p * cols, cols)
                normed[part, where] = (
                    arr[p, part].astype(f32) * factor * norm_ref[0:1, where]
                ).astype(bf16)
            return carry

        lax.fori_loop(0, unit_rows // n_rows, norm_step, 0)
        rows = pl.ds(unit * unit_rows, unit_rows)

        def gate_step(i, carry):
            where = pl.ds(pl.multiple_of(i * tile_f, tile_f), tile_f)
            gate = dot(normed[rows], wg[:, where])
            up = dot(normed[rows], wu[:, where])
            hid_all[t, rows, where] = (gate / (1.0 + jnp.exp(-gate)) * up).astype(bf16)
            return carry

        lax.fori_loop(0, hidden_w // tile_f, gate_step, 0)
        tp_send(hid_all, hid_sems, 2, unit)

    expert_in(0)
    expert_in(1)
    lax.fori_loop(1, 2, kv_attend, 0)

    @pl.when(z + 1 < n_z)
    def _():
        lax.fori_loop(2, n_z - 1, kv_pass, 0)

    tp_hand_on(hid_all, hid_sems, 2, 0)
    tp_hand_on(hid_all, hid_sems, 2, 1)
    tile_o = min(out_w, 256)

    def expert_out(unit):
        tp_arrive(hid_all, hid_sems, 2, unit)
        rows = pl.ds(unit * unit_rows, unit_rows)

        def down_step(i, carry):
            where = pl.ds(pl.multiple_of(i * tile_o, tile_o), tile_o)
            total = dot(hid_all[0, rows], wd[pl.ds(0, hidden_w), where])
            for p in range(1, n_tp):
                total = total + dot(hid_all[p, rows], wd[pl.ds(p * hidden_w, hidden_w), where])
            out_e[rows, where] = total.astype(bf16)
            return carry

        lax.fori_loop(0, out_w // tile_o, down_step, 0)
        ret_each(unit, lambda copy: copy.start())

    expert_out(0)
    expert_out(1)
    ret[pl.ds(pl.multiple_of(e * cap, cap), cap)] = out_e[pl.ds(first_slot(z, 0), cap)]

    def kv_late(s, carry):
        @pl.when(z + 1 == n_z)
        def _():
            kv_pass(s, 0)

        return kv_attend(s, carry)

    lax.fori_loop(2, n_z, kv_late, 0)

    def head_step(h, carry):
        first = acc[h, pl.ds(0, n_tok)] / run_sum[h, pl.ds(0, n_tok)]
        second = acc[h, pl.ds(n_tok, n_tok)] / run_sum[h, pl.ds(n_tok, n_tok)]
        mixed = first - scale_ref[h] * second
        mean_sq = jnp.mean(mixed * mixed, axis=-1, keepdims=True)
        head_all[t, :, pl.ds(pl.multiple_of(h * val_w, val_w), val_w)] = (
            mixed * lax.rsqrt(mean_sq + eps) * gain_ref[0:1] * head_factor
        ).astype(bf16)
        return carry

    lax.fori_loop(0, per_head, head_step, 0)
    tp_send(head_all, head_sems, 1, 0)

    row_of = lax.broadcasted_iota(jnp.int32, (tok_b, tok_b), 0)
    col_of = lax.broadcasted_iota(jnp.int32, (tok_b, tok_b), 1)

    def column(row):
        return jnp.sum(
            jnp.where(row_of == col_of, row.astype(f32), 0.0), axis=1, keepdims=True
        )

    shares = []
    for k in range(route_count):
        ids = column(ids_ref[k : k + 1])
        same = jnp.zeros((tok_b, tok_b), f32)
        for other in range(route_count):
            same = same + (ids_ref[other : other + 1].astype(f32) == ids).astype(f32)
        ranks = jnp.sum(jnp.where(col_of < row_of, same, 0.0), axis=1, keepdims=True)
        slot = lax.broadcasted_iota(jnp.int32, (tok_b, slots), 1).astype(f32)
        spread[k] = jnp.where(slot == ids * cap + ranks, 1.0, 0.0).astype(bf16)
        shares.append(column(route_w_ref[k : k + 1]))

    tp_hand_on(head_all, head_sems, 1, 0)
    tp_arrive(head_all, head_sems, 1, 0)
    heads_w = head_all.shape[2]

    def mixer_step(i, carry):
        where = pl.ds(pl.multiple_of(i * tile_o, tile_o), tile_o)
        total = dot(head_all[0], wo[pl.ds(0, heads_w), where])
        for p in range(1, n_tp):
            total = total + dot(head_all[p], wo[pl.ds(p * heads_w, heads_w), where])
        mixer_ref[:, where] = total.astype(bf16)
        return carry

    lax.fori_loop(0, out_w // tile_o, mixer_step, 0)

    each_ep(lambda b: ret_arrival(b).wait_recv())
    tile_m = min(out_w, 256)
    for start in range(0, out_w, tile_m):
        where = pl.ds(start, tile_m)
        total = shares[0] * dot(spread[0], ret[:, where])
        for k in range(1, route_count):
            total = total + shares[k] * dot(spread[k], ret[:, where])
        mix_ref[:, where] = total.astype(bf16)

    each_ep(lambda to: ids_copy(to).wait_send())
    for unit in range(2):
        ret_each(unit, lambda copy: copy.wait_send())
    tp_drain(arr, arr_sems, 2)
    tp_drain(hid_all, hid_sems, 2)
    tp_drain(head_all, head_sems, 1)

    def drain(j, carry):
        rows_copy_side(j).wait_send()

        @pl.when((j <= z) & (z + 1 < n_z))
        def _():
            rows_copy_up(j).wait_send()
            for copy in kv_copies_up(j):
                copy.wait_send()

        @pl.when((j >= z) & (z > 0))
        def _():
            rows_copy_down(j).wait_send()

        @pl.when((j < z) | ((j == z) & (c == 0)))
        def _():
            for copy in kv_copies_side(j):
                copy.wait_send()

        return carry

    lax.fori_loop(0, n_z, drain, 0)


def per_device(
    n_ep,
    n_tp,
    query_rows,
    key_rows,
    value_rows,
    second_scale,
    head_gain,
    out_weight,
    routed_rows,
    norm_gain,
    route_ids,
    route_weight,
    expert_gate,
    expert_up,
    expert_down,
):
    n_tok, attn_w = query_rows.shape
    per_head = second_scale.shape[0]
    val_w = head_gain.shape[0]
    head_w = attn_w // per_head
    tok_b, cols = routed_rows.shape
    route_count = route_ids.shape[1]
    hidden_w = expert_gate.shape[2]
    out_w = out_weight.shape[1]
    n_z = n_ep // lanes
    cap = 2 * tok_b * route_count // n_ep
    slots = n_ep * cap
    vmem = pl.BlockSpec(memory_space=pltpu.VMEM)
    hbm = pl.BlockSpec(memory_space=pl.ANY)
    dma = pltpu.SemaphoreType.DMA
    return pl.pallas_call(
        functools.partial(layer_kernel, n_ep, n_tp),
        out_shape=(
            jax.ShapeDtypeStruct((n_tok, out_w), bf16),
            jax.ShapeDtypeStruct((tok_b, out_w), bf16),
        ),
        in_specs=[
            pl.BlockSpec(memory_space=pltpu.SMEM),
            hbm,
            hbm,
            hbm,
            vmem,
            hbm,
            hbm,
            vmem,
            vmem,
            vmem,
            hbm,
            hbm,
            hbm,
        ],
        out_specs=(vmem, vmem),
        scratch_shapes=[
            pltpu.VMEM((n_tok, attn_w), bf16),
            pltpu.VMEM((per_head, 2 * n_tok, head_w), bf16),
            pltpu.VMEM((n_ep, n_tok, attn_w), bf16),
            pltpu.VMEM((n_ep, n_tok, value_rows.shape[1]), bf16),
            pltpu.VMEM((n_ep, tok_b, cols), bf16),
            pltpu.VMEM((n_ep, 8, tok_b), jnp.int32),
            pltpu.VMEM((n_tp, slots, cols), bf16),
            pltpu.VMEM((slots, n_tp * cols), bf16),
            pltpu.VMEM((n_tp, slots, hidden_w), bf16),
            pltpu.VMEM((slots, out_w), bf16),
            pltpu.VMEM((slots, out_w), bf16),
            pltpu.VMEM((n_tp, n_tok, per_head * val_w), bf16),
            pltpu.VMEM((route_count, tok_b, slots), bf16),
            pltpu.VMEM((per_head, 2 * n_tok, val_w), f32),
            pltpu.VMEM((per_head, 2 * n_tok, 1), f32),
            pltpu.VMEM((per_head, 2 * n_tok, 1), f32),
            pltpu.VMEM(expert_gate.shape[1:], bf16),
            pltpu.VMEM(expert_up.shape[1:], bf16),
            pltpu.VMEM(expert_down.shape[1:], bf16),
            pltpu.VMEM(out_weight.shape, bf16),
            dma((4,)),
            dma((4,)),
            dma((n_z,)),
            dma((n_z,)),
            dma((n_z,)),
            dma((n_ep,)),
            dma((n_ep,)),
            dma((n_ep,)),
            dma((2, n_z)),
            dma((2, n_z)),
            dma((2, n_ep)),
            dma((n_tp, 4)),
            dma((n_tp, 4)),
            dma((n_tp, 4)),
            dma((n_tp, 4)),
            dma((n_tp, 2)),
            dma((n_tp, 2)),
            dma((n_ep,)),
            dma((n_ep,)),
        ],
        compiler_params=pltpu.CompilerParams(
            collective_id=0, has_side_effects=True, vmem_limit_bytes=66000000
        ),
    )(
        second_scale,
        query_rows,
        key_rows,
        value_rows,
        head_gain.reshape(1, -1),
        out_weight,
        routed_rows,
        norm_gain.reshape(1, -1),
        route_ids.T,
        route_weight.T,
        expert_gate,
        expert_up,
        expert_down,
    )


def solution(mesh):
    placed = (
        P("ep", "tp"),
        P("ep", "tp"),
        P("ep", "tp"),
        P("tp"),
        P(),
        P(None, "tp"),
        P("ep", "tp"),
        P(),
        P("ep", None),
        P("ep", None),
        P("ep", None, "tp"),
        P("ep", None, "tp"),
        P("ep", None, "tp"),
    )
    return jax.shard_map(
        functools.partial(per_device, mesh.shape["ep"], mesh.shape["tp"]),
        mesh=mesh,
        in_specs=placed,
        out_specs=(P("ep", "tp"), P("ep", "tp")),
        check_vma=False,
    )
```

profile of v0, /device:TPU:24, one launch (start us, length us, event | category | flops | bytes accessed | tf_op | source)
XLA Modules:
  0.0 122.2 jit_solution(1850558242295395666)
XLA Ops:
  0.6 117.8 %shard_map.140 = (bf16[384,1024]{1,0:T(8,128)(2,1)}, bf16[128,1024]{1,0:T(8,128)(2,1)}) custom-call(f32[4]{0:T(128)} %scale_ref.1, bf16[384,512]{1,0:T(8,128)(2,1)} %q_hbm.1, bf16[384,512]{1,0:T(8,128)(2,1)} %k_hbm.1, bf16[384,512]{1,0:T(8,128)(2,1)} %v_hbm.1, f32[1,128]{1,0:T(1,128)} %bitcast.7, bf16[2048,1024]{1,0:T(8,128)(2,1)} %wo_hbm.1, ...), custom_call_target="tpu_custom_call" | custom-call | tf_op jit(solution)/shard_map/pallas_call | solution.py:647
  118.4 2.1 %copy.17 = bf16[384,1024]{1,0:T(8,128)(2,1)} copy(bf16[384,1024]{1,0:T(8,128)(2,1)} %get-tuple-element.4) | data formatting | bytes 1572864
  120.5 1.7 %copy.18 = bf16[128,1024]{1,0:T(8,128)(2,1)} copy(bf16[128,1024]{1,0:T(8,128)(2,1)} %get-tuple-element.5) | data formatting | bytes 524288
where the time goes:
time: 122 us
  Pallas kernels  118 us (97%)
  local copies, waits for them, and re-layouts  3.73 us (3%)
    pallas_call x1, Pallas kernels, per_device(): pl.pallas_call(functools.partial(layer_kernel, n_ep, n_tp), out_shape=(ja...  118 us
    unnamed x2, local copies, waits for them, and re-layouts  3.73 us

commit v1 on v0

--- a/solution.py
+++ b/solution.py
@@ -38,6 +38,7 @@
     mixer_ref,
     mix_ref,
     q_in,
+    q_far,
     q_two,
     k_all,
     v_all,
@@ -53,6 +54,10 @@
     acc,
     run_max,
     run_sum,
+    lse_own,
+    lse_far,
+    part_out,
+    part_in,
     wg,
     wu,
     wd,
@@ -65,9 +70,13 @@
     rows_recv,
     ids_send,
     ids_recv,
-    kv_up,
+    kv_out,
     kv_side,
     kv_recv,
+    far_send,
+    far_recv,
+    part_send,
+    part_recv,
     arr_send,
     arr_recv,
     hid_send,
@@ -85,12 +94,14 @@
     partner = z * lanes + (1 - c)
     n_tok = q_in.shape[0]
     tok_b = rows_all.shape[1]
-    per_head = acc.shape[0]
+    per_head = scale_ref.shape[0]
     head_w = q_two.shape[2]
-    val_w = acc.shape[2]
+    val_w = acc.shape[1]
     slots, out_w = ret.shape
     cap = slots // n_ep
     half = n_z // 2
+    upper = z >= half
+    far = lax.rem(z + half, n_z) * lanes + c
     cols = arr.shape[2]
     hidden_w = hid_all.shape[2]
     route_count = ids_ref.shape[0]
@@ -105,10 +116,13 @@
             device_id_type=pl.DeviceIdType.MESH,
         )
 
+    def kv_part(ref, j, core):
+        return ref.at[j, pl.ds(pl.multiple_of(core * n_tok, n_tok), n_tok)]
+
     loads = [
         pltpu.make_async_copy(rows_hbm, rows_all.at[e], local_sem.at[0]),
-        pltpu.make_async_copy(k_hbm, k_all.at[e], local_sem.at[1]),
-        pltpu.make_async_copy(v_hbm, v_all.at[e], local_sem.at[2]),
+        pltpu.make_async_copy(k_hbm, kv_part(k_all, z, c), local_sem.at[1]),
+        pltpu.make_async_copy(v_hbm, kv_part(v_all, z, c), local_sem.at[2]),
         pltpu.make_async_copy(q_hbm, q_in, local_sem.at[3]),
     ]
     for load in loads:
@@ -157,24 +171,54 @@
     def rows_copy_side(j):
         return rows_copy(j * lanes + c, rows_side.at[j], partner)
 
-    def kv_copies(j, sems, to):
-        block = j * lanes + c
+    def kv_copies(j, core, sems, at, to):
         return [
-            remote(ref.at[block], ref.at[block], sems.at[i, j], kv_recv.at[i, block], to, t)
+            remote(
+                kv_part(ref, j, core),
+                kv_part(ref, j, core),
+                sems.at[i, at],
+                kv_recv.at[i, j * lanes + core],
+                to,
+                t,
+            )
             for i, ref in enumerate((k_all, v_all))
         ]
 
-    def kv_copies_up(j):
-        return kv_copies(j, kv_up, lax.rem(e + lanes, n_ep))
+    def kv_copies_out(j):
+        return kv_copies(z, c, kv_out, j, j * lanes + c)
 
     def kv_copies_side(j):
-        return kv_copies(j, kv_side, partner)
-
-    def kv_wait(block):
-        for i, ref in enumerate((k_all, v_all)):
-            remote(
-                ref.at[block], ref.at[block], kv_up.at[i, 0], kv_recv.at[i, block], partner, t
-            ).wait_recv()
+        return kv_copies(j, c, kv_side, j, partner)
+
+    def kv_sent_to(j):
+        return ((z < half) & (j < half) & (j != z)) | ((z >= half) & (j > z))
+
+    def kv_got_from(j):
+        return ((z < half) & (j < half) & (j != z)) | ((j >= half) & (j < z))
+
+    def kv_wait(j, core):
+        for copy in kv_copies(j, core, kv_side, j, partner):
+            copy.wait_recv()
+
+    def each_z(first, last, cond, work):
+        def one(j, carry):
+            @pl.when(cond(j))
+            def _():
+                work(j)
+
+            return carry
+
+        lax.fori_loop(first, last, one, 0)
+
+    def start_all(copies):
+        for copy in copies:
+            copy.start()
+
+    q_copy = remote(q_in, q_far, far_send.at[0], far_recv.at[0], far, t)
+    lse_copy = remote(lse_own, lse_far, far_send.at[1], far_recv.at[1], far, t)
+
+    def part_copy(h):
+        return remote(part_out.at[h], part_in.at[h], part_send.at[h], part_recv.at[h], far, t)
 
     square = n_tp == 4
     across = t + 1 - 2 * lax.rem(t, 2)
@@ -322,15 +366,18 @@
         def _():
             rows_copy_down(high).start()
 
-        @pl.when((s == z) & (z + 1 < n_z))
-        def _():
-            for copy in kv_copies_up(z):
-                copy.start()
-
-        @pl.when((s == z) & (c == 0))
-        def _():
-            for copy in kv_copies_side(z):
-                copy.start()
+        @pl.when(s == z)
+        def _():
+            each_z(z + 1, n_z, kv_sent_to, lambda j: start_all(kv_copies_out(j)))
+            start_all(kv_copies_side(z))
+
+        @pl.when((s == n_z - 1 - z) & upper)
+        def _():
+            q_copy.start()
+
+        @pl.when((s == n_z - 1 - z) & (z < half))
+        def _():
+            each_z(0, z, kv_sent_to, lambda j: start_all(kv_copies_out(j)))
 
         @pl.when(low >= 0)
         def _():
@@ -369,88 +416,98 @@
 
     lane = lax.broadcasted_iota(jnp.int32, (n_tok, head_w), 1)
 
-    def split_maps(h, carry):
-        scaled = q_in[:, pl.ds(pl.multiple_of(h * head_w, head_w), head_w)].astype(f32) * (
-            (head_w // 2) ** -0.5
-        )
-        q_two[h, pl.ds(0, n_tok)] = jnp.where(lane < head_w // 2, scaled, 0.0).astype(bf16)
-        q_two[h, pl.ds(n_tok, n_tok)] = jnp.where(lane < head_w // 2, 0.0, scaled).astype(bf16)
-        return carry
-
-    lax.fori_loop(0, per_head, split_maps, 0)
-
-    def attend(block, own):
+    def split_maps(ref, base):
         def one(h, carry):
-            keys = k_all[block, :, pl.ds(pl.multiple_of(h * head_w, head_w), head_w)]
-            values = v_all[block, :, pl.ds(pl.multiple_of(h * val_w, val_w), val_w)]
-            for m in range(2):
-                part = pl.ds(m * n_tok, n_tok)
+            scaled = ref[:, pl.ds(pl.multiple_of(h * head_w, head_w), head_w)].astype(f32) * (
+                (head_w // 2) ** -0.5
+            )
+            q_two[base + h, pl.ds(0, n_tok)] = jnp.where(lane < head_w // 2, scaled, 0.0).astype(bf16)
+            q_two[base + h, pl.ds(n_tok, n_tok)] = jnp.where(lane < head_w // 2, 0.0, scaled).astype(bf16)
+            return carry
+
+        lax.fori_loop(0, per_head, one, 0)
+
+    def attend(base, j, keys_at, n_keys, first, own):
+        def one(h, carry):
+            slot = base + h
+            keys = k_all[j, pl.ds(keys_at, n_keys), pl.ds(pl.multiple_of(h * head_w, head_w), head_w)]
+            values = v_all[j, pl.ds(keys_at, n_keys), pl.ds(pl.multiple_of(h * val_w, val_w), val_w)].T
+
+            def score(m):
                 scores = lax.dot_general(
-                    q_two[h, part], keys, (((1,), (1,)), ((), ())), preferred_element_type=f32
+                    keys,
+                    q_two[slot, pl.ds(m * n_tok, n_tok)],
+                    (((1,), (1,)), ((), ())),
+                    preferred_element_type=f32,
                 )
                 if own:
                     scores = jnp.where(
-                        lax.broadcasted_iota(jnp.int32, (n_tok, n_tok), 0)
-                        >= lax.broadcasted_iota(jnp.int32, (n_tok, n_tok), 1),
+                        lax.broadcasted_iota(jnp.int32, (n_keys, n_tok), 0)
+                        <= lax.broadcasted_iota(jnp.int32, (n_keys, n_tok), 1),
                         scores,
                         neg_big,
                     )
-                top = jnp.max(scores, axis=-1, keepdims=True)
-                if not own:
-                    old = run_max[h, part]
+                return scores
+
+            both = [score(m) for m in range(2)]
+            for m in range(2):
+                part = pl.ds(m * n_tok, n_tok)
+                scores = both[m]
+                top = jnp.max(scores, axis=0, keepdims=True)
+                if not first:
+                    old = run_max[slot, :, part]
                     top = jnp.maximum(old, top)
                 shares = jnp.exp(scores - top)
-                total = jnp.sum(shares, axis=-1, keepdims=True)
-                update = dot(shares.astype(bf16), values)
-                if not own:
+                total = jnp.sum(shares, axis=0, keepdims=True)
+                update = dot(values, shares.astype(bf16))
+                if not first:
                     shrink = jnp.exp(old - top)
-                    total = total + run_sum[h, part] * shrink
-                    update = update + acc[h, part] * shrink
-                run_max[h, part] = top
-                run_sum[h, part] = total
-                acc[h, part] = update
+                    total = total + run_sum[slot, :, part] * shrink
+                    update = update + acc[slot, :, part] * shrink
+                run_max[slot, :, part] = top
+                run_sum[slot, :, part] = total
+                acc[slot, :, part] = update
             return carry
 
         lax.fori_loop(0, per_head, one, 0)
 
-    attend(e, True)
+    def attend_chip(base, j, first):
+        attend(base, j, 0, lanes * n_tok, first, False)
+
+    def core_at(core):
+        return pl.multiple_of(core * n_tok, n_tok)
+
+    split_maps(q_in, 0)
+    attend(0, z, core_at(c), n_tok, True, True)
+    kv_wait(z, 1 - c)
 
     @pl.when(c == 1)
     def _():
-        kv_wait(partner)
-        attend(partner, False)
+        attend(0, z, core_at(1 - c), n_tok, False, False)
 
     tp_hand_on(arr, arr_sems, 2, 1)
 
-    def kv_pass(s, carry):
-        j = z - s
-
-        @pl.when(j >= 0)
-        def _():
-            kv_wait(j * lanes + c)
-
-            @pl.when(z + 1 < n_z)
-            def _():
-                for copy in kv_copies_up(j):
-                    copy.start()
-
-            for copy in kv_copies_side(j):
-                copy.start()
-
-        return carry
-
-    def kv_attend(s, carry):
-        j = z - s
-
-        @pl.when(j >= 0)
-        def _():
-            attend(j * lanes + c, False)
-            kv_wait(j * lanes + (1 - c))
-            attend(j * lanes + (1 - c), False)
-
-        return carry
-
-    lax.fori_loop(1, 2, kv_pass, 0)
+    def kv_arrive(j):
+        kv_wait(j, c)
+        start_all(kv_copies_side(j))
+
+    def put_lse(base):
+        for h in range(per_head):
+            total = run_max[base + h] + jnp.log(run_sum[base + h])
+            for m in range(2):
+                lse_own[2 * h + m : 2 * h + m + 1] = total[:, m * n_tok : (m + 1) * n_tok]
+
+    def mixed_maps(base, h, shared):
+        maps = []
+        for m in range(2):
+            part = pl.ds(m * n_tok, n_tok)
+            weight = 1.0 / run_sum[base + h, :, part]
+            if shared:
+                row = pl.ds(2 * h + m, 1)
+                weight = weight / (1.0 + jnp.exp(lse_far[row] - lse_own[row]))
+            maps.append((acc[base + h, :, part], weight))
+        (first, first_w), (second, second_w) = maps
+        return first * first_w - second * (second_w * scale_ref[h])
 
     for weight in weights:
         weight.wait()
@@ -489,12 +546,44 @@
         tp_send(hid_all, hid_sems, 2, unit)
 
     expert_in(0)
+
+    @pl.when(z < half)
+    def _():
+        q_copy.wait_recv()
+        split_maps(q_far, per_head)
+        attend_chip(per_head, z, True)
+
+    each_z(0, n_z, kv_got_from, kv_arrive)
+
+    @pl.when(z < half)
+    def _():
+        def one(j):
+            kv_wait(j, 1 - c)
+            attend_chip(per_head, j, False)
+
+        each_z(0, half, kv_got_from, one)
+        put_lse(per_head)
+        lse_copy.start()
+
+    @pl.when(upper)
+    def _():
+        def one(j):
+            kv_wait(j, 1 - c)
+            attend_chip(0, j, False)
+
+        each_z(half, n_z, kv_got_from, one)
+        put_lse(0)
+        lse_copy.start()
+
     expert_in(1)
-    lax.fori_loop(1, 2, kv_attend, 0)
-
-    @pl.when(z + 1 < n_z)
+
+    @pl.when(z < half)
     def _():
-        lax.fori_loop(2, n_z - 1, kv_pass, 0)
+        lse_copy.wait_recv()
+        for h in range(per_head):
+            part_out[h] = mixed_maps(per_head, h, True).astype(bf16)
+            part_copy(h).start()
+        each_z(0, z, kv_got_from, lambda j: attend_chip(0, j, False))
 
     tp_hand_on(hid_all, hid_sems, 2, 0)
     tp_hand_on(hid_all, hid_sems, 2, 1)
@@ -519,26 +608,23 @@
     expert_out(1)
     ret[pl.ds(pl.multiple_of(e * cap, cap), cap)] = out_e[pl.ds(first_slot(z, 0), cap)]
 
-    def kv_late(s, carry):
-        @pl.when(z + 1 == n_z)
-        def _():
-            kv_pass(s, 0)
-
-        return kv_attend(s, carry)
-
-    lax.fori_loop(2, n_z, kv_late, 0)
-
-    def head_step(h, carry):
-        first = acc[h, pl.ds(0, n_tok)] / run_sum[h, pl.ds(0, n_tok)]
-        second = acc[h, pl.ds(n_tok, n_tok)] / run_sum[h, pl.ds(n_tok, n_tok)]
-        mixed = first - scale_ref[h] * second
-        mean_sq = jnp.mean(mixed * mixed, axis=-1, keepdims=True)
-        head_all[t, :, pl.ds(pl.multiple_of(h * val_w, val_w), val_w)] = (
-            mixed * lax.rsqrt(mean_sq + eps) * gain_ref[0:1] * head_factor
-        ).astype(bf16)
-        return carry
-
-    lax.fori_loop(0, per_head, head_step, 0)
+    def head_step(h, mixed):
+        mean_sq = jnp.mean(mixed * mixed, axis=0, keepdims=True)
+        normal = mixed * lax.rsqrt(mean_sq + eps) * gain_ref[...] * head_factor
+        head_all[t, :, h * val_w : (h + 1) * val_w] = normal.T.astype(bf16)
+
+    @pl.when(z < half)
+    def _():
+        for h in range(per_head):
+            head_step(h, mixed_maps(0, h, False))
+
+    @pl.when(upper)
+    def _():
+        lse_copy.wait_recv()
+        for h in range(per_head):
+            part_copy(h).wait_recv()
+            head_step(h, mixed_maps(0, h, True) + part_in[h].astype(f32))
+
     tp_send(head_all, head_sems, 1, 0)
 
     row_of = lax.broadcasted_iota(jnp.int32, (tok_b, tok_b), 0)
@@ -596,14 +682,17 @@
         @pl.when((j <= z) & (z + 1 < n_z))
         def _():
             rows_copy_up(j).wait_send()
-            for copy in kv_copies_up(j):
+
+        @pl.when((j >= z) & (z > 0))
+        def _():
+            rows_copy_down(j).wait_send()
+
+        @pl.when(kv_sent_to(j))
+        def _():
+            for copy in kv_copies_out(j):
                 copy.wait_send()
 
-        @pl.when((j >= z) & (z > 0))
-        def _():
-            rows_copy_down(j).wait_send()
-
-        @pl.when((j < z) | ((j == z) & (c == 0)))
+        @pl.when((j == z) | kv_got_from(j))
         def _():
             for copy in kv_copies_side(j):
                 copy.wait_send()
@@ -611,6 +700,16 @@
         return carry
 
     lax.fori_loop(0, n_z, drain, 0)
+    lse_copy.wait_send()
+
+    @pl.when(upper)
+    def _():
+        q_copy.wait_send()
+
+    @pl.when(z < half)
+    def _():
+        for h in range(per_head):
+            part_copy(h).wait_send()
 
 
 def per_device(
@@ -668,9 +767,10 @@
         out_specs=(vmem, vmem),
         scratch_shapes=[
             pltpu.VMEM((n_tok, attn_w), bf16),
-            pltpu.VMEM((per_head, 2 * n_tok, head_w), bf16),
-            pltpu.VMEM((n_ep, n_tok, attn_w), bf16),
-            pltpu.VMEM((n_ep, n_tok, value_rows.shape[1]), bf16),
+            pltpu.VMEM((n_tok, attn_w), bf16),
+            pltpu.VMEM((2 * per_head, 2 * n_tok, head_w), bf16),
+            pltpu.VMEM((n_z, lanes * n_tok, attn_w), bf16),
+            pltpu.VMEM((n_z, lanes * n_tok, value_rows.shape[1]), bf16),
             pltpu.VMEM((n_ep, tok_b, cols), bf16),
             pltpu.VMEM((n_ep, 8, tok_b), jnp.int32),
             pltpu.VMEM((n_tp, slots, cols), bf16),
@@ -680,9 +780,13 @@
             pltpu.VMEM((slots, out_w), bf16),
             pltpu.VMEM((n_tp, n_tok, per_head * val_w), bf16),
             pltpu.VMEM((route_count, tok_b, slots), bf16),
-            pltpu.VMEM((per_head, 2 * n_tok, val_w), f32),
-            pltpu.VMEM((per_head, 2 * n_tok, 1), f32),
-            pltpu.VMEM((per_head, 2 * n_tok, 1), f32),
+            pltpu.VMEM((2 * per_head, val_w, 2 * n_tok), f32),
+            pltpu.VMEM((2 * per_head, 1, 2 * n_tok), f32),
+            pltpu.VMEM((2 * per_head, 1, 2 * n_tok), f32),
+            pltpu.VMEM((2 * per_head, n_tok), f32),
+            pltpu.VMEM((2 * per_head, n_tok), f32),
+            pltpu.VMEM((per_head, val_w, n_tok), bf16),
+            pltpu.VMEM((per_head, val_w, n_tok), bf16),
             pltpu.VMEM(expert_gate.shape[1:], bf16),
             pltpu.VMEM(expert_up.shape[1:], bf16),
             pltpu.VMEM(expert_down.shape[1:], bf16),
@@ -698,6 +802,10 @@
             dma((2, n_z)),
             dma((2, n_z)),
             dma((2, n_ep)),
+            dma((2,)),
+            dma((2,)),
+            dma((per_head,)),
+            dma((per_head,)),
             dma((n_tp, 4)),
             dma((n_tp, 4)),
             dma((n_tp, 4)),
@@ -715,7 +823,7 @@
         query_rows,
         key_rows,
         value_rows,
-        head_gain.reshape(1, -1),
+        head_gain.reshape(-1, 1),
         out_weight,
         routed_rows,
         norm_gain.reshape(1, -1),

time: 122 us -> 117 us (0.959)
  the two profiles are of different devices: /device:TPU:24 before, /device:TPU:1 now
where the time goes in v1:
time: 117 us
  Pallas kernels  111 us (95%)
  local copies, waits for them, and re-layouts  5.12 us (4%)
    pallas_call x1, Pallas kernels, per_device(): pl.pallas_call(functools.partial(layer_kernel, n_ep, n_tp), out_shape=(ja...  111 us
    unnamed x2, local copies, waits for them, and re-layouts  3.73 us

profile of v1, /device:TPU:1, one launch (start us, length us, event | category | flops | bytes accessed | tf_op | source)
XLA Modules:
  0.0 116.9 jit_solution(8630924634578842080)
XLA Ops:
  0.6 1.4 %copy.15.gain_ref = f32[128,1]{1,0:T(8,128)} copy(f32[128,1]{0,1:T(1,128)} %bitcast.7) | data formatting | bytes 1024 | tf_op jit(solution)/shard_map/reshape | solution.py:826
  2.0 111.2 %shard_map.140 = (bf16[384,1024]{1,0:T(8,128)(2,1)}, bf16[128,1024]{1,0:T(8,128)(2,1)}) custom-call(f32[4]{0:T(128)} %scale_ref.1, bf16[384,512]{1,0:T(8,128)(2,1)} %q_hbm.1, bf16[384,512]{1,0:T(8,128)(2,1)} %k_hbm.1, bf16[384,512]{1,0:T(8,128)(2,1)} %v_hbm.1, f32[128,1]{1,0:T(8,128)} %copy.15.gain_ref, bf16[2048,1024]{1,0:T(8,128)(2,1)} %wo_hbm.1, ...), custom_call_target="tpu_custom_call" | custom-call | tf_op jit(solution)/shard_map/pallas_call | solution.py:746
  113.2 2.1 %copy.18 = bf16[384,1024]{1,0:T(8,128)(2,1)} copy(bf16[384,1024]{1,0:T(8,128)(2,1)} %get-tuple-element.4) | data formatting | bytes 1572864
  115.3 1.7 %copy.19 = bf16[128,1024]{1,0:T(8,128)(2,1)} copy(bf16[128,1024]{1,0:T(8,128)(2,1)} %get-tuple-element.5) | data formatting | bytes 524288

commit v2 on v1

--- a/solution.py
+++ b/solution.py
@@ -75,6 +75,8 @@
     kv_recv,
     far_send,
     far_recv,
+    lse_send,
+    lse_recv,
     part_send,
     part_recv,
     arr_send,
@@ -100,8 +102,9 @@
     slots, out_w = ret.shape
     cap = slots // n_ep
     half = n_z // 2
-    upper = z >= half
-    far = lax.rem(z + half, n_z) * lanes + c
+    upper = z >= n_z - 2
+    worker = (z >= n_z - 4) & (z < n_z - 2)
+    far = jnp.where(upper, z - 2, lax.rem(z + 2, n_z)) * lanes + c
     cols = arr.shape[2]
     hidden_w = hid_all.shape[2]
     route_count = ids_ref.shape[0]
@@ -149,9 +152,10 @@
 
     lax.fori_loop(1, n_ep, greet_ep, 0)
     lax.fori_loop(1, n_tp, greet_tp, 0)
-    pl.semaphore_wait(barrier, n_ep - 1 + n_tp - 1)
-    for load in loads:
-        load.wait()
+    with jax.named_scope("barrier"):
+        pl.semaphore_wait(barrier, n_ep - 1 + n_tp - 1)
+        for load in loads:
+            load.wait()
 
     def ids_copy(to):
         return remote(ids_all.at[e], ids_all.at[e], ids_send.at[to], ids_recv.at[e], to, t)
@@ -191,10 +195,10 @@
         return kv_copies(j, c, kv_side, j, partner)
 
     def kv_sent_to(j):
-        return ((z < half) & (j < half) & (j != z)) | ((z >= half) & (j > z))
+        return (j > z) & ((j < n_z - 2) | (j == z + 1))
 
     def kv_got_from(j):
-        return ((z < half) & (j < half) & (j != z)) | ((j >= half) & (j < z))
+        return (j < z) & ((z < n_z - 2) | (j == z - 1))
 
     def kv_wait(j, core):
         for copy in kv_copies(j, core, kv_side, j, partner):
@@ -214,8 +218,10 @@
         for copy in copies:
             copy.start()
 
-    q_copy = remote(q_in, q_far, far_send.at[0], far_recv.at[0], far, t)
-    lse_copy = remote(lse_own, lse_far, far_send.at[1], far_recv.at[1], far, t)
+    q_copy = remote(q_in, q_far, far_send, far_recv, far, t)
+
+    def lse_copy(h):
+        return remote(lse_own.at[h], lse_far.at[h], lse_send.at[h], lse_recv.at[h], far, t)
 
     def part_copy(h):
         return remote(part_out.at[h], part_in.at[h], part_send.at[h], part_recv.at[h], far, t)
@@ -226,6 +232,10 @@
     corner = n_tp - 1 - t
 
     def piece(buf, source, i, units):
+        if buf is head_all:
+            step = n_tok // 2
+            cols_at = pl.ds((i // 2) * val_w, val_w)
+            return buf.at[source, pl.ds((i % 2) * step, step), cols_at]
         step = buf.shape[1] // (2 * units)
         return buf.at[source, pl.ds(i * step, step)]
 
@@ -347,6 +357,14 @@
             ).start()
         )
 
+    def rows_left_up(j, carry):
+        rows_copy_up(j).wait_send()
+        return carry
+
+    def rows_left_down(j, carry):
+        rows_copy_down(j).wait_send()
+        return carry
+
     def rows_step(s, carry):
         low, high = z - s, z + s
 
@@ -366,18 +384,16 @@
         def _():
             rows_copy_down(high).start()
 
-        @pl.when(s == z)
-        def _():
-            each_z(z + 1, n_z, kv_sent_to, lambda j: start_all(kv_copies_out(j)))
+        @pl.when(s == 1)
+        def _():
             start_all(kv_copies_side(z))
-
-        @pl.when((s == n_z - 1 - z) & upper)
-        def _():
-            q_copy.start()
-
-        @pl.when((s == n_z - 1 - z) & (z < half))
-        def _():
-            each_z(0, z, kv_sent_to, lambda j: start_all(kv_copies_out(j)))
+            for weight in weights:
+                weight.start()
+
+        @pl.when(s == z + 1)
+        def _():
+            lax.fori_loop(0, s, rows_left_up, 0)
+            each_z(s, n_z, kv_sent_to, lambda j: start_all(kv_copies_out(j)))
 
         @pl.when(low >= 0)
         def _():
@@ -386,6 +402,16 @@
         @pl.when((s > 0) & (high < n_z))
         def _():
             rows_copy_side(high).start()
+
+        @pl.when(s == half)
+        def _():
+            @pl.when(upper)
+            def _():
+                lax.fori_loop(z, n_z, rows_left_down, 0)
+                q_copy.start()
+
+            with jax.named_scope("arr_hand0"):
+                tp_hand_on(arr, arr_sems, 2, 0)
 
         def take(j):
             mine, other = j * lanes + c, j * lanes + (1 - c)
@@ -399,21 +425,24 @@
             rows_copy(other, rows_side.at[j], partner).wait_recv()
             pick(other, j, 1)
 
+        up_first = z >= half
+
+        @pl.when(up_first & (s > 0) & (high < n_z))
+        def _():
+            take(high)
+
         @pl.when(low >= 0)
         def _():
             take(low)
 
-        @pl.when((s > 0) & (high < n_z))
+        @pl.when(jnp.logical_not(up_first) & (s > 0) & (high < n_z))
         def _():
             take(high)
 
         return carry
 
-    lax.fori_loop(0, n_z, rows_step, 0)
-    for weight in weights:
-        weight.start()
-    tp_hand_on(arr, arr_sems, 2, 0)
-
+    with jax.named_scope("rows"):
+        lax.fori_loop(0, n_z, rows_step, 0)
     lane = lax.broadcasted_iota(jnp.int32, (n_tok, head_w), 1)
 
     def split_maps(ref, base):
@@ -427,7 +456,7 @@
 
         lax.fori_loop(0, per_head, one, 0)
 
-    def attend(base, j, keys_at, n_keys, first, own):
+    def attend(base, j, keys_at, n_keys, first, own, then=None):
         def one(h, carry):
             slot = base + h
             keys = k_all[j, pl.ds(keys_at, n_keys), pl.ds(pl.multiple_of(h * head_w, head_w), head_w)]
@@ -467,35 +496,43 @@
                 run_max[slot, :, part] = top
                 run_sum[slot, :, part] = total
                 acc[slot, :, part] = update
+            if then is not None:
+                then(h)
             return carry
 
         lax.fori_loop(0, per_head, one, 0)
 
-    def attend_chip(base, j, first):
-        attend(base, j, 0, lanes * n_tok, first, False)
+    def attend_chip(base, j, first, then=None):
+        with jax.named_scope("attend_chip"):
+            attend(base, j, 0, lanes * n_tok, first, False, then)
 
     def core_at(core):
         return pl.multiple_of(core * n_tok, n_tok)
 
-    split_maps(q_in, 0)
-    attend(0, z, core_at(c), n_tok, True, True)
-    kv_wait(z, 1 - c)
+    with jax.named_scope("own"):
+        split_maps(q_in, 0)
+        attend(0, z, core_at(c), n_tok, True, True)
+        kv_wait(z, 1 - c)
 
     @pl.when(c == 1)
     def _():
         attend(0, z, core_at(1 - c), n_tok, False, False)
 
-    tp_hand_on(arr, arr_sems, 2, 1)
-
     def kv_arrive(j):
-        kv_wait(j, c)
+        with jax.named_scope("kv_wait"):
+            kv_wait(j, c)
         start_all(kv_copies_side(j))
 
-    def put_lse(base):
-        for h in range(per_head):
-            total = run_max[base + h] + jnp.log(run_sum[base + h])
-            for m in range(2):
-                lse_own[2 * h + m : 2 * h + m + 1] = total[:, m * n_tok : (m + 1) * n_tok]
+    def put_lse(base, h):
+        total = run_max[base + h] + jnp.log(run_sum[base + h])
+        for m in range(2):
+            lse_own[h, m : m + 1] = total[:, m * n_tok : (m + 1) * n_tok]
+        lse_copy(h).start()
+
+    def part_step(h):
+        lse_copy(h).wait_recv()
+        part_out[h] = mixed_maps(per_head, h, True).astype(bf16)
+        part_copy(h).start()
 
     def mixed_maps(base, h, shared):
         maps = []
@@ -503,20 +540,22 @@
             part = pl.ds(m * n_tok, n_tok)
             weight = 1.0 / run_sum[base + h, :, part]
             if shared:
-                row = pl.ds(2 * h + m, 1)
-                weight = weight / (1.0 + jnp.exp(lse_far[row] - lse_own[row]))
+                row = pl.ds(m, 1)
+                weight = weight / (1.0 + jnp.exp(lse_far[h, row] - lse_own[h, row]))
             maps.append((acc[base + h, :, part], weight))
         (first, first_w), (second, second_w) = maps
         return first * first_w - second * (second_w * scale_ref[h])
 
-    for weight in weights:
-        weight.wait()
+    with jax.named_scope("w_wait"):
+        for weight in weights:
+            weight.wait()
     unit_rows = slots // 2
     n_rows = min(unit_rows, 64)
     tile_f = min(hidden_w, 256)
 
     def expert_in(unit):
-        tp_arrive(arr, arr_sems, 2, unit)
+        with jax.named_scope("arr_arrive"):
+            tp_arrive(arr, arr_sems, 2, unit)
 
         def norm_step(i, carry):
             part = pl.ds(pl.multiple_of(unit * unit_rows + i * n_rows, n_rows), n_rows)
@@ -532,7 +571,8 @@
                 ).astype(bf16)
             return carry
 
-        lax.fori_loop(0, unit_rows // n_rows, norm_step, 0)
+        with jax.named_scope("norm"):
+            lax.fori_loop(0, unit_rows // n_rows, norm_step, 0)
         rows = pl.ds(unit * unit_rows, unit_rows)
 
         def gate_step(i, carry):
@@ -542,55 +582,73 @@
             hid_all[t, rows, where] = (gate / (1.0 + jnp.exp(-gate)) * up).astype(bf16)
             return carry
 
-        lax.fori_loop(0, hidden_w // tile_f, gate_step, 0)
-        tp_send(hid_all, hid_sems, 2, unit)
+        with jax.named_scope("gate"):
+            lax.fori_loop(0, hidden_w // tile_f, gate_step, 0)
+
+    def kv_wait_other(j):
+        with jax.named_scope("kv_wait2"):
+            kv_wait(j, 1 - c)
 
     expert_in(0)
-
-    @pl.when(z < half)
-    def _():
-        q_copy.wait_recv()
+    with jax.named_scope("arr_hand1"):
+        tp_hand_on(arr, arr_sems, 2, 1)
+    tp_send(hid_all, hid_sems, 2, 0)
+
+    @pl.when(worker)
+    def _():
+        with jax.named_scope("q_wait"):
+            q_copy.wait_recv()
         split_maps(q_far, per_head)
         attend_chip(per_head, z, True)
 
-    each_z(0, n_z, kv_got_from, kv_arrive)
-
-    @pl.when(z < half)
-    def _():
-        def one(j):
-            kv_wait(j, 1 - c)
-            attend_chip(per_head, j, False)
-
-        each_z(0, half, kv_got_from, one)
-        put_lse(per_head)
-        lse_copy.start()
-
-    @pl.when(upper)
-    def _():
-        def one(j):
-            kv_wait(j, 1 - c)
-            attend_chip(0, j, False)
-
-        each_z(half, n_z, kv_got_from, one)
-        put_lse(0)
-        lse_copy.start()
+    def near_own():
+        kv_wait_other(z - 1)
+        attend_chip(0, z - 1, False, lambda h: put_lse(0, h))
+
+    @pl.when(z == n_z - 2)
+    def _():
+        kv_arrive(z - 1)
+        near_own()
+
+    @pl.when(z != n_z - 2)
+    def _():
+        each_z(0, n_z, kv_got_from, kv_arrive)
+
+    @pl.when(z == n_z - 1)
+    def _():
+        near_own()
+
+    @pl.when(z < n_z - 2)
+    def _():
+        each_z(0, n_z, kv_got_from, kv_wait_other)
+
+    @pl.when(worker)
+    def _():
+        each_z(0, z, kv_got_from, lambda j: attend_chip(per_head, j, False))
+
+        for h in range(per_head):
+            put_lse(per_head, h)
+
+    @pl.when(worker & (z != n_z - 3))
+    def _():
+        for h in range(per_head):
+            part_step(h)
 
     expert_in(1)
-
-    @pl.when(z < half)
-    def _():
-        lse_copy.wait_recv()
+    with jax.named_scope("hid_hand0"):
+        tp_hand_on(hid_all, hid_sems, 2, 0)
+    tp_send(hid_all, hid_sems, 2, 1)
+
+    @pl.when(z == n_z - 3)
+    def _():
         for h in range(per_head):
-            part_out[h] = mixed_maps(per_head, h, True).astype(bf16)
-            part_copy(h).start()
-        each_z(0, z, kv_got_from, lambda j: attend_chip(0, j, False))
-
-    tp_hand_on(hid_all, hid_sems, 2, 0)
-    tp_hand_on(hid_all, hid_sems, 2, 1)
+            part_step(h)
+
     tile_o = min(out_w, 256)
 
     def expert_out(unit):
-        tp_arrive(hid_all, hid_sems, 2, unit)
+        with jax.named_scope("hid_arrive"):
+            tp_arrive(hid_all, hid_sems, 2, unit)
         rows = pl.ds(unit * unit_rows, unit_rows)
 
         def down_step(i, carry):
@@ -601,31 +659,41 @@
             out_e[rows, where] = total.astype(bf16)
             return carry
 
-        lax.fori_loop(0, out_w // tile_o, down_step, 0)
+        with jax.named_scope("down"):
+            lax.fori_loop(0, out_w // tile_o, down_step, 0)
         ret_each(unit, lambda copy: copy.start())
 
     expert_out(0)
+
+    @pl.when(z < n_z - 2)
+    def _():
+        each_z(0, z, kv_got_from, lambda j: attend_chip(0, j, False))
+
+    with jax.named_scope("hid_hand1"):
+        tp_hand_on(hid_all, hid_sems, 2, 1)
     expert_out(1)
     ret[pl.ds(pl.multiple_of(e * cap, cap), cap)] = out_e[pl.ds(first_slot(z, 0), cap)]
 
+    gain = jnp.broadcast_to(gain_ref[...], (8, val_w)).T[:, 0:1]
+
     def head_step(h, mixed):
         mean_sq = jnp.mean(mixed * mixed, axis=0, keepdims=True)
-        normal = mixed * lax.rsqrt(mean_sq + eps) * gain_ref[...] * head_factor
+        normal = mixed * lax.rsqrt(mean_sq + eps) * gain * head_factor
         head_all[t, :, h * val_w : (h + 1) * val_w] = normal.T.astype(bf16)
-
-    @pl.when(z < half)
+        tp_send(head_all, head_sems, per_head, h)
+
+    @pl.when(z < n_z - 2)
     def _():
         for h in range(per_head):
             head_step(h, mixed_maps(0, h, False))
 
     @pl.when(upper)
     def _():
-        lse_copy.wait_recv()
         for h in range(per_head):
-            part_copy(h).wait_recv()
+            lse_copy(h).wait_recv()
+            with jax.named_scope("part_wait"):
+                part_copy(h).wait_recv()
             head_step(h, mixed_maps(0, h, True) + part_in[h].astype(f32))
-
-    tp_send(head_all, head_sems, 1, 0)
 
     row_of = lax.broadcasted_iota(jnp.int32, (tok_b, tok_b), 0)
     col_of = lax.broadcasted_iota(jnp.int32, (tok_b, tok_b), 1)
@@ -646,8 +714,11 @@
         spread[k] = jnp.where(slot == ids * cap + ranks, 1.0, 0.0).astype(bf16)
         shares.append(column(route_w_ref[k : k + 1]))
 
-    tp_hand_on(head_all, head_sems, 1, 0)
-    tp_arrive(head_all, head_sems, 1, 0)
+    with jax.named_scope("head_x"):
+        for h in range(per_head):
+            tp_hand_on(head_all, head_sems, per_head, h)
+        for h in range(per_head):
+            tp_arrive(head_all, head_sems, per_head, h)
     heads_w = head_all.shape[2]
 
     def mixer_step(i, carry):
@@ -658,9 +729,11 @@
         mixer_ref[:, where] = total.astype(bf16)
         return carry
 
-    lax.fori_loop(0, out_w // tile_o, mixer_step, 0)
-
-    each_ep(lambda b: ret_arrival(b).wait_recv())
+    with jax.named_scope("mixer"):
+        lax.fori_loop(0, out_w // tile_o, mixer_step, 0)
+
+    with jax.named_scope("ret_wait"):
+        each_ep(lambda b: ret_arrival(b).wait_recv())
     tile_m = min(out_w, 256)
     for start in range(0, out_w, tile_m):
         where = pl.ds(start, tile_m)
@@ -669,21 +742,18 @@
             total = total + shares[k] * dot(spread[k], ret[:, where])
         mix_ref[:, where] = total.astype(bf16)
 
-    each_ep(lambda to: ids_copy(to).wait_send())
+    with jax.named_scope("drain"):
+        each_ep(lambda to: ids_copy(to).wait_send())
     for unit in range(2):
         ret_each(unit, lambda copy: copy.wait_send())
     tp_drain(arr, arr_sems, 2)
     tp_drain(hid_all, hid_sems, 2)
-    tp_drain(head_all, head_sems, 1)
+    tp_drain(head_all, head_sems, per_head)
 
     def drain(j, carry):
         rows_copy_side(j).wait_send()
 
-        @pl.when((j <= z) & (z + 1 < n_z))
-        def _():
-            rows_copy_up(j).wait_send()
-
-        @pl.when((j >= z) & (z > 0))
+        @pl.when((j >= z) & (z > 0) & (z < n_z - 2))
         def _():
             rows_copy_down(j).wait_send()
 
@@ -700,13 +770,17 @@
         return carry
 
     lax.fori_loop(0, n_z, drain, 0)
-    lse_copy.wait_send()
 
     @pl.when(upper)
     def _():
         q_copy.wait_send()
 
-    @pl.when(z < half)
+    @pl.when(upper | worker)
+    def _():
+        for h in range(per_head):
+            lse_copy(h).wait_send()
+
+    @pl.when(worker)
     def _():
         for h in range(per_head):
             part_copy(h).wait_send()
@@ -783,8 +857,8 @@
             pltpu.VMEM((2 * per_head, val_w, 2 * n_tok), f32),
             pltpu.VMEM((2 * per_head, 1, 2 * n_tok), f32),
             pltpu.VMEM((2 * per_head, 1, 2 * n_tok), f32),
-            pltpu.VMEM((2 * per_head, n_tok), f32),
-            pltpu.VMEM((2 * per_head, n_tok), f32),
+            pltpu.VMEM((per_head, 2, n_tok), f32),
+            pltpu.VMEM((per_head, 2, n_tok), f32),
             pltpu.VMEM((per_head, val_w, n_tok), bf16),
             pltpu.VMEM((per_head, val_w, n_tok), bf16),
             pltpu.VMEM(expert_gate.shape[1:], bf16),
@@ -802,16 +876,18 @@
             dma((2, n_z)),
             dma((2, n_z)),
             dma((2, n_ep)),
-            dma((2,)),
-            dma((2,)),
+            dma,
+            dma,
+            dma((per_head,)),
+            dma((per_head,)),
             dma((per_head,)),
             dma((per_head,)),
             dma((n_tp, 4)),
             dma((n_tp, 4)),
             dma((n_tp, 4)),
             dma((n_tp, 4)),
-            dma((n_tp, 2)),
-            dma((n_tp, 2)),
+            dma((n_tp, 2 * per_head)),
+            dma((n_tp, 2 * per_head)),
             dma((n_ep,)),
             dma((n_ep,)),
         ],
@@ -823,7 +899,7 @@
         query_rows,
         key_rows,
         value_rows,
-        head_gain.reshape(-1, 1),
+        head_gain.reshape(1, -1),
         out_weight,
         routed_rows,
         norm_gain.reshape(1, -1),

time: 117 us -> 98.1 us (0.84)
  the two profiles are of different devices: /device:TPU:1 before, /device:TPU:24 now
where the time goes in v2:
time: 98.1 us; the launch traced here: 97.6 us
  Pallas kernels  93.2 us (95%)
  local copies, waits for them, and re-layouts  3.73 us (4%)
    pallas_call x1, Pallas kernels, per_device(): pl.pallas_call(functools.partial(layer_kernel, n_ep, n_tp), out_shape=(ja...  93.2 us
    unnamed x2, local copies, waits for them, and re-layouts  3.73 us

profile of v2, /device:TPU:24, one launch (start us, length us, event | category | flops | bytes accessed | tf_op | source)
XLA Modules:
  0.0 97.6 jit_solution(3664054054335017139)
XLA Ops:
  0.6 93.2 %shard_map.140 = (bf16[384,1024]{1,0:T(8,128)(2,1)}, bf16[128,1024]{1,0:T(8,128)(2,1)}) custom-call(f32[4]{0:T(128)} %scale_ref.1, bf16[384,512]{1,0:T(8,128)(2,1)} %q_hbm.1, bf16[384,512]{1,0:T(8,128)(2,1)} %k_hbm.1, bf16[384,512]{1,0:T(8,128)(2,1)} %v_hbm.1, f32[1,128]{1,0:T(1,128)} %bitcast.7, bf16[2048,1024]{1,0:T(8,128)(2,1)} %wo_hbm.1, ...), custom_call_target="tpu_custom_call" | custom-call | tf_op jit(solution)/shard_map/pallas_call | solution.py:820
  93.9 2.1 %copy.17 = bf16[384,1024]{1,0:T(8,128)(2,1)} copy(bf16[384,1024]{1,0:T(8,128)(2,1)} %get-tuple-element.4) | data formatting | bytes 1572864
  95.9 1.7 %copy.18 = bf16[128,1024]{1,0:T(8,128)(2,1)} copy(bf16[128,1024]{1,0:T(8,128)(2,1)} %get-tuple-element.5) | data formatting | bytes 524288

commit v3 on v2

--- a/solution.py
+++ b/solution.py
@@ -102,6 +102,7 @@
     slots, out_w = ret.shape
     cap = slots // n_ep
     half = n_z // 2
+    near = jnp.where(z < half, z, z - (half - 1))
     upper = z >= n_z - 2
     worker = (z >= n_z - 4) & (z < n_z - 2)
     far = jnp.where(upper, z - 2, lax.rem(z + 2, n_z)) * lanes + c
@@ -163,17 +164,23 @@
     def ids_arrival(b):
         return remote(ids_all.at[b], ids_all.at[b], ids_send.at[b], ids_recv.at[b], b, t)
 
-    def rows_copy(block, send, to):
-        return remote(rows_all.at[block], rows_all.at[block], send, rows_recv.at[block], to, t)
-
-    def rows_copy_up(j):
-        return rows_copy(j * lanes + c, rows_up.at[j], lax.rem(e + lanes, n_ep))
-
-    def rows_copy_down(j):
-        return rows_copy(j * lanes + c, rows_down.at[j], lax.rem(e + n_ep - lanes, n_ep))
-
-    def rows_copy_side(j):
-        return rows_copy(j * lanes + c, rows_side.at[j], partner)
+    def rows_copy(ref, block, send, recv, to):
+        return remote(ref, ref, send, recv, to, t)
+
+    def rows_part(j, k, sems, to):
+        block = j * lanes + c
+        ref = rows_all.at[block, pl.ds(k * (tok_b // 2), tok_b // 2)]
+        return rows_copy(ref, block, sems.at[j, k], rows_recv.at[block, k], to)
+
+    def rows_copy_up(j, k):
+        return rows_part(j, k, rows_up, lax.rem(e + lanes, n_ep))
+
+    def rows_copy_down(j, k):
+        return rows_part(j, k, rows_down, lax.rem(e + n_ep - lanes, n_ep))
+
+    def rows_copy_side(j, core):
+        block = j * lanes + core
+        return rows_copy(rows_all.at[block], block, rows_side.at[j], rows_recv.at[block, 0], partner)
 
     def kv_copies(j, core, sems, at, to):
         return [
@@ -288,10 +295,11 @@
     head_sems = (head_send, head_recv)
 
     def unit_of(j):
-        return lax.rem(lax.div(j, half) + lax.div(z, half), 2)
+        return jnp.where((j >= near) & (j < near + half), 0, 1)
 
     def first_slot(j, side):
-        return pl.multiple_of(((unit_of(j) * 2 + side) * half + lax.rem(j, half)) * cap, cap)
+        at = jnp.where(j < near, j, jnp.where(j < near + half, j - near, j - half))
+        return pl.multiple_of(((unit_of(j) * 2 + side) * half + at) * cap, cap)
 
     def ret_part(b):
         return ret.at[pl.ds(pl.multiple_of(b * cap, cap), cap)]
@@ -309,7 +317,7 @@
 
     def ret_each(unit, work):
         def one(i, carry):
-            j = lax.rem(lax.div(z, half) + unit, 2) * half + i
+            j = near + i if unit == 0 else jnp.where(i < near, i, i + half)
             if unit == 0:
 
                 @pl.when(j != z)
@@ -358,31 +366,35 @@
         )
 
     def rows_left_up(j, carry):
-        rows_copy_up(j).wait_send()
+        for k in range(2):
+            rows_copy_up(j, k).wait_send()
         return carry
 
     def rows_left_down(j, carry):
-        rows_copy_down(j).wait_send()
+        for k in range(2):
+            rows_copy_down(j, k).wait_send()
         return carry
 
     def rows_step(s, carry):
         low, high = z - s, z + s
 
-        @pl.when((s > 0) & (low >= 0))
-        def _():
-            rows_copy_down(low).wait_recv()
-
-        @pl.when((low >= 0) & (z + 1 < n_z))
-        def _():
-            rows_copy_up(low).start()
-
-        @pl.when((s > 0) & (high < n_z))
-        def _():
-            rows_copy_up(high).wait_recv()
-
-        @pl.when((high < n_z) & (z > 0))
-        def _():
-            rows_copy_down(high).start()
+        for k in range(2):
+
+            @pl.when((s > 0) & (low >= 0))
+            def _():
+                rows_copy_down(low, k).wait_recv()
+
+            @pl.when((low >= 0) & (z + 1 < n_z))
+            def _():
+                rows_copy_up(low, k).start()
+
+            @pl.when((s > 0) & (high < n_z))
+            def _():
+                rows_copy_up(high, k).wait_recv()
+
+            @pl.when((high < n_z) & (z > 0))
+            def _():
+                rows_copy_down(high, k).start()
 
         @pl.when(s == 1)
         def _():
@@ -397,11 +409,11 @@
 
         @pl.when(low >= 0)
         def _():
-            rows_copy_side(low).start()
+            rows_copy_side(low, c).start()
 
         @pl.when((s > 0) & (high < n_z))
         def _():
-            rows_copy_side(high).start()
+            rows_copy_side(high, c).start()
 
         @pl.when(s == half)
         def _():
@@ -422,10 +434,10 @@
 
             pick(mine, j, 0)
             ids_arrival(other).wait_recv()
-            rows_copy(other, rows_side.at[j], partner).wait_recv()
+            rows_copy_side(j, 1 - c).wait_recv()
             pick(other, j, 1)
 
-        up_first = z >= half
+        up_first = z < half
 
         @pl.when(up_first & (s > 0) & (high < n_z))
         def _():
@@ -456,51 +468,56 @@
 
         lax.fori_loop(0, per_head, one, 0)
 
+    at_once = 2 - per_head % 2
+
     def attend(base, j, keys_at, n_keys, first, own, then=None):
-        def one(h, carry):
-            slot = base + h
-            keys = k_all[j, pl.ds(keys_at, n_keys), pl.ds(pl.multiple_of(h * head_w, head_w), head_w)]
-            values = v_all[j, pl.ds(keys_at, n_keys), pl.ds(pl.multiple_of(h * val_w, val_w), val_w)].T
-
-            def score(m):
-                scores = lax.dot_general(
-                    keys,
-                    q_two[slot, pl.ds(m * n_tok, n_tok)],
-                    (((1,), (1,)), ((), ())),
-                    preferred_element_type=f32,
+        def score(h, m):
+            scores = lax.dot_general(
+                k_all[j, pl.ds(keys_at, n_keys), pl.ds(pl.multiple_of(h * head_w, head_w), head_w)],
+                q_two[base + h, pl.ds(m * n_tok, n_tok)],
+                (((1,), (1,)), ((), ())),
+                preferred_element_type=f32,
+            )
+            if own:
+                scores = jnp.where(
+                    lax.broadcasted_iota(jnp.int32, (n_keys, n_tok), 0)
+                    <= lax.broadcasted_iota(jnp.int32, (n_keys, n_tok), 1),
+                    scores,
+                    neg_big,
                 )
-                if own:
-                    scores = jnp.where(
-                        lax.broadcasted_iota(jnp.int32, (n_keys, n_tok), 0)
-                        <= lax.broadcasted_iota(jnp.int32, (n_keys, n_tok), 1),
-                        scores,
-                        neg_big,
-                    )
-                return scores
-
-            both = [score(m) for m in range(2)]
-            for m in range(2):
-                part = pl.ds(m * n_tok, n_tok)
-                scores = both[m]
-                top = jnp.max(scores, axis=0, keepdims=True)
-                if not first:
-                    old = run_max[slot, :, part]
-                    top = jnp.maximum(old, top)
-                shares = jnp.exp(scores - top)
-                total = jnp.sum(shares, axis=0, keepdims=True)
-                update = dot(values, shares.astype(bf16))
-                if not first:
-                    shrink = jnp.exp(old - top)
-                    total = total + run_sum[slot, :, part] * shrink
-                    update = update + acc[slot, :, part] * shrink
-                run_max[slot, :, part] = top
-                run_sum[slot, :, part] = total
-                acc[slot, :, part] = update
+            return scores
+
+        def some(i, carry):
+            group = [i * at_once + k for k in range(at_once)]
+            every = [[score(h, m) for m in range(2)] for h in group]
+            for h, both in zip(group, every):
+                slot = base + h
+                values = v_all[
+                    j, pl.ds(keys_at, n_keys), pl.ds(pl.multiple_of(h * val_w, val_w), val_w)
+                ].T
+                for m in range(2):
+                    part = pl.ds(m * n_tok, n_tok)
+                    scores = both[m]
+                    top = jnp.max(scores, axis=0, keepdims=True)
+                    if not first:
+                        old = run_max[slot, :, part]
+                        top = jnp.maximum(old, top)
+                    shares = jnp.exp(scores - top)
+                    total = jnp.sum(shares, axis=0, keepdims=True)
+                    update = dot(values, shares.astype(bf16))
+                    if not first:
+                        shrink = jnp.exp(old - top)
+                        total = total + run_sum[slot, :, part] * shrink
+                        update = update + acc[slot, :, part] * shrink
+                    run_max[slot, :, part] = top
+                    run_sum[slot, :, part] = total
+                    acc[slot, :, part] = update
             if then is not None:
-                then(h)
+                for h in group:
+                    then(h)
             return carry
 
-        lax.fori_loop(0, per_head, one, 0)
+        lax.fori_loop(0, per_head // at_once, some, 0)
 
     def attend_chip(base, j, first, then=None):
         with jax.named_scope("attend_chip"):
@@ -514,7 +531,9 @@
         attend(0, z, core_at(c), n_tok, True, True)
         kv_wait(z, 1 - c)
 
-    @pl.when(c == 1)
+    inner = (z > 0) & (z < n_z - 1)
+
+    @pl.when((c == 1) & inner)
     def _():
         attend(0, z, core_at(1 - c), n_tok, False, False)
 
@@ -594,6 +613,14 @@
         tp_hand_on(arr, arr_sems, 2, 1)
     tp_send(hid_all, hid_sems, 2, 0)
 
+    @pl.when((c == 1) & jnp.logical_not(inner))
+    def _():
+        attend(0, z, core_at(1 - c), n_tok, False, False)
+
+    @pl.when(z != n_z - 2)
+    def _():
+        each_z(0, n_z, kv_got_from, kv_arrive)
+
     @pl.when(worker)
     def _():
         with jax.named_scope("q_wait"):
@@ -609,10 +636,6 @@
     def _():
         kv_arrive(z - 1)
         near_own()
-
-    @pl.when(z != n_z - 2)
-    def _():
-        each_z(0, n_z, kv_got_from, kv_arrive)
 
     @pl.when(z == n_z - 1)
     def _():
@@ -663,16 +686,9 @@
             lax.fori_loop(0, out_w // tile_o, down_step, 0)
         ret_each(unit, lambda copy: copy.start())
 
-    expert_out(0)
-
     @pl.when(z < n_z - 2)
     def _():
         each_z(0, z, kv_got_from, lambda j: attend_chip(0, j, False))
-
-    with jax.named_scope("hid_hand1"):
-        tp_hand_on(hid_all, hid_sems, 2, 1)
-    expert_out(1)
-    ret[pl.ds(pl.multiple_of(e * cap, cap), cap)] = out_e[pl.ds(first_slot(z, 0), cap)]
 
     gain = jnp.broadcast_to(gain_ref[...], (8, val_w)).T[:, 0:1]
 
@@ -682,18 +698,38 @@
         head_all[t, :, h * val_w : (h + 1) * val_w] = normal.T.astype(bf16)
         tp_send(head_all, head_sems, per_head, h)
 
-    @pl.when(z < n_z - 2)
-    def _():
-        for h in range(per_head):
-            head_step(h, mixed_maps(0, h, False))
-
-    @pl.when(upper)
-    def _():
-        for h in range(per_head):
-            lse_copy(h).wait_recv()
-            with jax.named_scope("part_wait"):
-                part_copy(h).wait_recv()
-            head_step(h, mixed_maps(0, h, True) + part_in[h].astype(f32))
+    def heads(first, last):
+        @pl.when(z < n_z - 2)
+        def _():
+            for h in range(first, last):
+                head_step(h, mixed_maps(0, h, False))
+
+        @pl.when(upper)
+        def _():
+            for h in range(first, last):
+                lse_copy(h).wait_recv()
+                with jax.named_scope("part_wait"):
+                    part_copy(h).wait_recv()
+                head_step(h, mixed_maps(0, h, True) + part_in[h].astype(f32))
+
+    early = 0
+    expert_out(0)
+
+    @pl.when(z < n_z - 1)
+    def _():
+        heads(0, early)
+
+    with jax.named_scope("hid_hand1"):
+        tp_hand_on(hid_all, hid_sems, 2, 1)
+    expert_out(1)
+
+    @pl.when(z == n_z - 1)
+    def _():
+        heads(0, early)
+
+    heads(early, per_head)
+
+    ret[pl.ds(pl.multiple_of(e * cap, cap), cap)] = out_e[pl.ds(first_slot(z, 0), cap)]
 
     row_of = lax.broadcasted_iota(jnp.int32, (tok_b, tok_b), 0)
     col_of = lax.broadcasted_iota(jnp.int32, (tok_b, tok_b), 1)
@@ -717,6 +753,49 @@
     with jax.named_scope("head_x"):
         for h in range(per_head):
             tp_hand_on(head_all, head_sems, per_head, h)
+
+    with jax.named_scope("drain"):
+        each_ep(lambda to: ids_copy(to).wait_send())
+        tp_drain(arr, arr_sems, 2)
+        tp_drain(hid_all, hid_sems, 2)
+
+    def drain(j, carry):
+        rows_copy_side(j, c).wait_send()
+
+        @pl.when((j >= z) & (z > 0) & (z < n_z - 2))
+        def _():
+            for k in range(2):
+                rows_copy_down(j, k).wait_send()
+
+        @pl.when(kv_sent_to(j))
+        def _():
+            for copy in kv_copies_out(j):
+                copy.wait_send()
+
+        @pl.when((j == z) | kv_got_from(j))
+        def _():
+            for copy in kv_copies_side(j):
+                copy.wait_send()
+
+        return carry
+
+    lax.fori_loop(0, n_z, drain, 0)
+
+    @pl.when(upper)
+    def _():
+        q_copy.wait_send()
+
+    @pl.when(upper | worker)
+    def _():
+        for h in range(per_head):
+            lse_copy(h).wait_send()
+
+    @pl.when(worker)
+    def _():
+        for h in range(per_head):
+            part_copy(h).wait_send()
+
+    with jax.named_scope("head_a"):
         for h in range(per_head):
             tp_arrive(head_all, head_sems, per_head, h)
     heads_w = head_all.shape[2]
@@ -742,48 +821,9 @@
             total = total + shares[k] * dot(spread[k], ret[:, where])
         mix_ref[:, where] = total.astype(bf16)
 
-    with jax.named_scope("drain"):
-        each_ep(lambda to: ids_copy(to).wait_send())
     for unit in range(2):
         ret_each(unit, lambda copy: copy.wait_send())
-    tp_drain(arr, arr_sems, 2)
-    tp_drain(hid_all, hid_sems, 2)
     tp_drain(head_all, head_sems, per_head)
-
-    def drain(j, carry):
-        rows_copy_side(j).wait_send()
-
-        @pl.when((j >= z) & (z > 0) & (z < n_z - 2))
-        def _():
-            rows_copy_down(j).wait_send()
-
-        @pl.when(kv_sent_to(j))
-        def _():
-            for copy in kv_copies_out(j):
-                copy.wait_send()
-
-        @pl.when((j == z) | kv_got_from(j))
-        def _():
-            for copy in kv_copies_side(j):
-                copy.wait_send()
-
-        return carry
-
-    lax.fori_loop(0, n_z, drain, 0)
-
-    @pl.when(upper)
-    def _():
-        q_copy.wait_send()
-
-    @pl.when(upper | worker)
-    def _():
-        for h in range(per_head):
-            lse_copy(h).wait_send()
-
-    @pl.when(worker)
-    def _():
-        for h in range(per_head):
-            part_copy(h).wait_send()
 
 
 def per_device(
@@ -817,11 +857,11 @@
     vmem = pl.BlockSpec(memory_space=pltpu.VMEM)
     hbm = pl.BlockSpec(memory_space=pl.ANY)
     dma = pltpu.SemaphoreType.DMA
-    return pl.pallas_call(
+    results = pl.pallas_call(
         functools.partial(layer_kernel, n_ep, n_tp),
         out_shape=(
-            jax.ShapeDtypeStruct((n_tok, out_w), bf16),
-            jax.ShapeDtypeStruct((tok_b, out_w), bf16),
+            pltpu.VMEM((n_tok, out_w), bf16),
+            pltpu.VMEM((tok_b, out_w), bf16),
         ),
         in_specs=[
             pl.BlockSpec(memory_space=pltpu.SMEM),
@@ -867,10 +907,10 @@
             pltpu.VMEM(out_weight.shape, bf16),
             dma((4,)),
             dma((4,)),
+            dma((n_z, 2)),
+            dma((n_z, 2)),
             dma((n_z,)),
-            dma((n_z,)),
-            dma((n_z,)),
-            dma((n_ep,)),
+            dma((n_ep, 2)),
             dma((n_ep,)),
             dma((n_ep,)),
             dma((2, n_z)),
@@ -892,7 +932,7 @@
             dma((n_ep,)),
         ],
         compiler_params=pltpu.CompilerParams(
-            collective_id=0, has_side_effects=True, vmem_limit_bytes=66000000
+            collective_id=0, has_side_effects=True, vmem_limit_bytes=65000000
         ),
     )(
         second_scale,
@@ -909,6 +949,7 @@
         expert_up,
         expert_down,
     )
+    return results
 
 
 def solution(mesh):

time: 98.1 us -> 90.1 us (0.918)
  Pallas kernels: 93.2 us -> 87.1 us
  local copies, waits for them, and re-layouts: 3.73 us -> 1.58 us
    pallas_call x1, Pallas kernels: 93.2 us -> 87.1 us  [per_device(): pl.pallas_call(functools.partial(layer_kernel, n_ep, n_tp), out_shape=(pl...]
    unnamed x2, local copies, waits for them, and re-layouts: 3.73 us -> 1.58 us
where the time goes in v3:
time: 90.1 us; the launch traced here: 89.3 us
  Pallas kernels  87.1 us (97%)
  local copies, waits for them, and re-layouts  1.58 us (2%)
    pallas_call x1, Pallas kernels, per_device(): pl.pallas_call(functools.partial(layer_kernel, n_ep, n_tp), out_shape=(pl...  87.1 us

profile of v3, /device:TPU:24, one launch (start us, length us, event | category | flops | bytes accessed | tf_op | source)
XLA Modules:
  0.0 89.3 jit_solution(3294197705517853942)
XLA Ops:
  0.6 87.1 %shard_map.140 = (bf16[384,1024]{1,0:T(8,128)(2,1)S(1)}, bf16[128,1024]{1,0:T(8,128)(2,1)S(1)}) custom-call(f32[4]{0:T(128)} %scale_ref.1, bf16[384,512]{1,0:T(8,128)(2,1)} %q_hbm.1, bf16[384,512]{1,0:T(8,128)(2,1)} %k_hbm.1, bf16[384,512]{1,0:T(8,128)(2,1)} %v_hbm.1, f32[1,128]{1,0:T(1,128)} %bitcast.7, bf16[2048,1024]{1,0:T(8,128)(2,1)} %wo_hbm.1, ...), custom_call_target="tpu_custom_call" | custom-call | tf_op jit(solution)/shard_map/pallas_call | solution.py:860
  87.7 0.9 copy.17
  88.6 0.7 copy.18

commit v4 on v3

--- a/solution.py
+++ b/solution.py
@@ -51,6 +51,7 @@
     ret,
     head_all,
     spread,
+    mixer_sum,
     acc,
     run_max,
     run_sum,
@@ -609,6 +610,11 @@
             kv_wait(j, 1 - c)
 
     expert_in(0)
+
+    @pl.when(z == n_z - 2)
+    def _():
+        kv_arrive(z - 1)
+
     with jax.named_scope("arr_hand1"):
         tp_hand_on(arr, arr_sems, 2, 1)
     tp_send(hid_all, hid_sems, 2, 0)
@@ -634,7 +640,6 @@
 
     @pl.when(z == n_z - 2)
     def _():
-        kv_arrive(z - 1)
         near_own()
 
     @pl.when(z == n_z - 1)
@@ -654,8 +659,9 @@
 
     @pl.when(worker & (z != n_z - 3))
     def _():
-        for h in range(per_head):
-            part_step(h)
+        with jax.named_scope("part"):
+            for h in range(per_head):
+                part_step(h)
 
     expert_in(1)
     with jax.named_scope("hid_hand0"):
@@ -712,22 +718,11 @@
                     part_copy(h).wait_recv()
                 head_step(h, mixed_maps(0, h, True) + part_in[h].astype(f32))
 
-    early = 0
     expert_out(0)
-
-    @pl.when(z < n_z - 1)
-    def _():
-        heads(0, early)
-
     with jax.named_scope("hid_hand1"):
         tp_hand_on(hid_all, hid_sems, 2, 1)
+    heads(0, per_head)
     expert_out(1)
-
-    @pl.when(z == n_z - 1)
-    def _():
-        heads(0, early)
-
-    heads(early, per_head)
 
     ret[pl.ds(pl.multiple_of(e * cap, cap), cap)] = out_e[pl.ds(first_slot(z, 0), cap)]
 
@@ -754,6 +749,36 @@
         for h in range(per_head):
             tp_hand_on(head_all, head_sems, per_head, h)
 
+    heads_w = head_all.shape[2]
+    groups = per_head // at_once
+    group_w = heads_w // groups
+
+    def mixer_group(g):
+        with jax.named_scope("head_a"):
+            for h in range(g * at_once, (g + 1) * at_once):
+                tp_arrive(head_all, head_sems, per_head, h)
+
+        def step(i, carry):
+            where = pl.ds(pl.multiple_of(i * tile_o, tile_o), tile_o)
+            total = mixer_sum[:, where] if g > 0 else None
+            for p in range(n_tp):
+                more = dot(
+                    head_all[p, :, g * group_w : (g + 1) * group_w],
+                    wo[pl.ds(p * heads_w + g * group_w, group_w), where],
+                )
+                total = more if total is None else total + more
+            if g < groups - 1:
+                mixer_sum[:, where] = total
+            else:
+                mixer_ref[:, where] = total.astype(bf16)
+            return carry
+
+        with jax.named_scope("mixer"):
+            lax.fori_loop(0, out_w // tile_o, step, 0)
+
+    for g in range(groups - 1):
+        mixer_group(g)
+
     with jax.named_scope("drain"):
         each_ep(lambda to: ids_copy(to).wait_send())
         tp_drain(arr, arr_sems, 2)
@@ -795,35 +820,23 @@
         for h in range(per_head):
             part_copy(h).wait_send()
 
-    with jax.named_scope("head_a"):
-        for h in range(per_head):
-            tp_arrive(head_all, head_sems, per_head, h)
-    heads_w = head_all.shape[2]
-
-    def mixer_step(i, carry):
-        where = pl.ds(pl.multiple_of(i * tile_o, tile_o), tile_o)
-        total = dot(head_all[0], wo[pl.ds(0, heads_w), where])
-        for p in range(1, n_tp):
-            total = total + dot(head_all[p], wo[pl.ds(p * heads_w, heads_w), where])
-        mixer_ref[:, where] = total.astype(bf16)
-        return carry
-
-    with jax.named_scope("mixer"):
-        lax.fori_loop(0, out_w // tile_o, mixer_step, 0)
-
+    mixer_group(groups - 1)
+
+    with jax.named_scope("head_d"):
+        ret_each(0, lambda copy: copy.wait_send())
+        tp_drain(head_all, head_sems, per_head)
     with jax.named_scope("ret_wait"):
         each_ep(lambda b: ret_arrival(b).wait_recv())
-    tile_m = min(out_w, 256)
-    for start in range(0, out_w, tile_m):
-        where = pl.ds(start, tile_m)
-        total = shares[0] * dot(spread[0], ret[:, where])
-        for k in range(1, route_count):
-            total = total + shares[k] * dot(spread[k], ret[:, where])
-        mix_ref[:, where] = total.astype(bf16)
-
-    for unit in range(2):
-        ret_each(unit, lambda copy: copy.wait_send())
-    tp_drain(head_all, head_sems, per_head)
+    with jax.named_scope("mix"):
+        tile_m = min(out_w, 256)
+        for start in range(0, out_w, tile_m):
+            where = pl.ds(start, tile_m)
+            total = shares[0] * dot(spread[0], ret[:, where])
+            for k in range(1, route_count):
+                total = total + shares[k] * dot(spread[k], ret[:, where])
+            mix_ref[:, where] = total.astype(bf16)
+
+    ret_each(1, lambda copy: copy.wait_send())
 
 
 def per_device(
@@ -894,6 +907,7 @@
             pltpu.VMEM((slots, out_w), bf16),
             pltpu.VMEM((n_tp, n_tok, per_head * val_w), bf16),
             pltpu.VMEM((route_count, tok_b, slots), bf16),
+            pltpu.VMEM((n_tok, out_w), f32),
             pltpu.VMEM((2 * per_head, val_w, 2 * n_tok), f32),
             pltpu.VMEM((2 * per_head, 1, 2 * n_tok), f32),
             pltpu.VMEM((2 * per_head, 1, 2 * n_tok), f32),

time: 90.1 us -> 89.4 us (level)
  no operation moved by 1% of the time
where the time goes in v4:
time: 89.4 us; the launch traced here: 88.8 us
  Pallas kernels  86.6 us (97%)
  local copies, waits for them, and re-layouts  1.58 us (2%)
    pallas_call x1, Pallas kernels, per_device(): pl.pallas_call(functools.partial(layer_kernel, n_ep, n_tp), out_shape=(pl...  86.6 us

profile of v4, /device:TPU:24, one launch (start us, length us, event | category | flops | bytes accessed | tf_op | source)
XLA Modules:
  0.0 88.8 jit_solution(16973020400957120620)
XLA Ops:
  0.6 86.6 %shard_map.140 = (bf16[384,1024]{1,0:T(8,128)(2,1)S(1)}, bf16[128,1024]{1,0:T(8,128)(2,1)S(1)}) custom-call(f32[4]{0:T(128)} %scale_ref.1, bf16[384,512]{1,0:T(8,128)(2,1)} %q_hbm.1, bf16[384,512]{1,0:T(8,128)(2,1)} %k_hbm.1, bf16[384,512]{1,0:T(8,128)(2,1)} %v_hbm.1, f32[1,128]{1,0:T(1,128)} %bitcast.7, bf16[2048,1024]{1,0:T(8,128)(2,1)} %wo_hbm.1, ...), custom_call_target="tpu_custom_call" | custom-call | tf_op jit(solution)/shard_map/pallas_call | solution.py:873
  87.3 0.9 copy.17
  88.1 0.7 copy.18
